TPU v7x, 32 devices: a whole 2x2x4 slice. The times are simulated.
32 devices in a mesh: sp: 16 (over z, y, core), tp: 2 (over x).
Axes of the slice: x: 2, y: 2, z: 4, core: 2. Of those that a mesh axis runs over, the one named last changes fastest.
Arguments:
- block_input: bfloat16 [6144, 2048], P('sp'), may hold values from -6 to 6
- proj_x: bfloat16 [2048, 1024], P(None, 'tp'), may hold values from -0.125 to 0.125
- proj_gate: bfloat16 [2048, 1024], P(None, 'tp'), may hold values from -0.125 to 0.125
- conv_taps: float32 [4, 1024], P(None, 'tp'), may hold values from -3 to 3
- gate_a: bfloat16 [16, 64, 64], P('tp'), may hold values from -0.75 to 0.75
- gate_in: bfloat16 [16, 64, 64], P('tp'), may hold values from -0.75 to 0.75
- decay_param: float32 [1024], P('tp'), may hold values from 3 to 30
- log_jump: float32 [6144, 1024], P('sp', 'tp'), may hold values from -1 to 0, as said below
- out_grad: bfloat16 [6144, 1024], P('sp', 'tp'), may hold values from -6 to 6
Outputs:
- grad_input: bfloat16 [6144, 2048], P(('sp', 'tp'))
- grad_proj: float32 [2048, 1024], P('sp', 'tp')
Inputs may be any that keep to these rules, and one draw needn't show every extreme that they name: `log_jump`: strictly negative.
All inputs are finite; a program needn't handle non-finite values.
Results may differ from a plain program's by a relative error of at most 0.015.
Values may be sent and summed in bfloat16 or wider, within the bound.
A program may use at most 64 MiB of HBM per device.

v0:
```python
import jax
import jax.numpy as jnp
from jax import lax
from jax.sharding import PartitionSpec as P

gate_power = 8.0


def from_behind(x, axis, by):
    count = lax.axis_size(axis)
    pairs = [(i, i + by) for i in range(count) if 0 <= i + by < count]
    return lax.ppermute(x, axis, pairs)


def prefix(x, axis, combine, identity, reverse):
    count, here = (lax.axis_size(axis), lax.axis_index(axis))
    everything = jax.tree.map(lambda part: lax.all_gather(part, axis), x)
    start = jax.tree.map(
        lambda part, zero: jnp.broadcast_to(jnp.asarray(zero, part.dtype), part.shape), x, identity
    )

    def lap(k, before):
        at = count - 1 - k if reverse else k
        reached = at > here if reverse else at < here
        new = combine(before, jax.tree.map(lambda part: part[at], everything))
        return jax.tree.map(lambda a, b: jnp.where(reached, a, b), new, before)

    return lax.fori_loop(0, count, lap, start)


def combine(earlier, later):
    return (earlier[0] * later[0], later[0] * earlier[1] + later[1])


def body(
    block_input, proj_x, proj_gate, conv_taps, gate_a, gate_in, decay_param, log_jump, out_grad
):
    tok_rows = block_input.shape[0]
    chan_width = proj_x.shape[1]
    tap_count = conv_taps.shape[0]
    block_count = gate_a.shape[0]
    block_width = gate_a.shape[1]
    branch = jnp.dot(block_input, proj_x, preferred_element_type=jnp.float32).astype(jnp.bfloat16)
    gate_pre = jnp.dot(block_input, proj_gate, preferred_element_type=jnp.float32).astype(
        jnp.bfloat16
    )
    tail = from_behind(branch[tok_rows - tap_count + 1 :], "sp", 1)
    extended = jnp.concatenate([tail, branch], axis=0).astype(jnp.float32)
    mixed_sum = jnp.zeros((tok_rows, chan_width), jnp.float32)
    for offset in range(tap_count):
        mixed_sum = mixed_sum + conv_taps[offset][None, :] * extended[offset : offset + tok_rows]
    mixed = mixed_sum.astype(jnp.bfloat16)
    mixed_f = mixed.astype(jnp.float32)
    mixed_blocks = mixed.reshape(tok_rows, block_count, block_width)
    rec_gate = jax.nn.sigmoid(
        jnp.einsum(
            "tbi,bij->tbj", mixed_blocks, gate_a, preferred_element_type=jnp.float32
        ).reshape(tok_rows, chan_width)
    )
    in_gate = jax.nn.sigmoid(
        jnp.einsum(
            "tbi,bij->tbj", mixed_blocks, gate_in, preferred_element_type=jnp.float32
        ).reshape(tok_rows, chan_width)
    )
    log_sig = jax.nn.log_sigmoid(decay_param)
    log_decay = gate_power * rec_gate * log_sig[None, :] + log_jump
    decays = jnp.exp(log_decay)
    square_decay = jnp.exp(2.0 * log_decay)
    norm_factor = jnp.sqrt(-jnp.expm1(2.0 * log_decay))
    drive = norm_factor * in_gate * mixed_f
    running_decay, hidden_local = lax.associative_scan(combine, (decays, drive), axis=0)
    activation, pullback = jax.vjp(jax.nn.gelu, gate_pre.astype(jnp.float32))
    grad_out = out_grad.astype(jnp.float32)
    grad_hidden = grad_out * activation
    next_decay = jnp.concatenate([decays[1:], jnp.ones((1, chan_width), jnp.float32)], axis=0)
    suffix_flip, grad_flip = lax.associative_scan(
        combine, (next_decay[::-1], grad_hidden[::-1]), axis=0
    )
    suffix_prod = suffix_flip[::-1]
    grad_local = grad_flip[::-1]
    total_decay = running_decay[-1]
    forward_end = hidden_local[-1]
    reverse_start = decays[0] * grad_local[0]
    identity = (jnp.ones((chan_width,), jnp.float32), jnp.zeros((chan_width,), jnp.float32))
    state_in = prefix((total_decay, forward_end), "sp", combine, identity, False)[1]
    carry_in = prefix((total_decay, reverse_start), "sp", combine, identity, True)[1]
    hidden = hidden_local + running_decay * state_in[None, :]
    grad_state = grad_local + suffix_prod * carry_in[None, :]
    hidden_prev = jnp.concatenate([state_in[None, :], hidden[:-1]], axis=0)
    grad_log = (
        grad_state * hidden_prev * decays
        - grad_state * in_gate * mixed_f * square_decay / norm_factor
    )
    grad_pre_a = (grad_log * gate_power * log_sig[None, :] * rec_gate * (1.0 - rec_gate)).astype(
        jnp.bfloat16
    )
    grad_pre_in = (grad_state * norm_factor * mixed_f * in_gate * (1.0 - in_gate)).astype(
        jnp.bfloat16
    )
    back_a = jnp.einsum(
        "tbj,bij->tbi",
        grad_pre_a.reshape(tok_rows, block_count, block_width),
        gate_a,
        preferred_element_type=jnp.float32,
    )
    back_in = jnp.einsum(
        "tbj,bij->tbi",
        grad_pre_in.reshape(tok_rows, block_count, block_width),
        gate_in,
        preferred_element_type=jnp.float32,
    )
    grad_mixed = grad_state * norm_factor * in_gate + (back_a + back_in).reshape(
        tok_rows, chan_width
    )
    head = from_behind(grad_mixed[: tap_count - 1], "sp", -1)
    extended_grad = jnp.concatenate([grad_mixed, head], axis=0)
    branch_sum = jnp.zeros((tok_rows, chan_width), jnp.float32)
    for offset in range(tap_count):
        start = tap_count - 1 - offset
        branch_sum = (
            branch_sum + conv_taps[offset][None, :] * extended_grad[start : start + tok_rows]
        )
    grad_branch = branch_sum.astype(jnp.bfloat16)
    stored_hidden = lax.optimization_barrier(hidden.astype(jnp.bfloat16)).astype(jnp.float32)
    grad_gate = pullback(grad_out * stored_hidden)[0].astype(jnp.bfloat16)
    grad_proj = lax.psum_scatter(
        lax.dot_general(
            block_input, grad_branch, (((0,), (0,)), ((), ())), preferred_element_type=jnp.float32
        ),
        "sp",
        scatter_dimension=0,
        tiled=True,
    )
    term = lax.dot_general(
        grad_branch, proj_x, (((1,), (1,)), ((), ())), preferred_element_type=jnp.float32
    )
    summed = lax.psum_scatter(
        (
            term
            + lax.dot_general(
                grad_gate, proj_gate, (((1,), (1,)), ((), ())), preferred_element_type=jnp.float32
            )
        ).astype(jnp.bfloat16),
        "tp",
        scatter_dimension=0,
        tiled=True,
    )
    return (summed, grad_proj)


def solution(mesh):
    in_specs = (
        P("sp", None),
        P(None, "tp"),
        P(None, "tp"),
        P(None, "tp"),
        P("tp", None, None),
        P("tp", None, None),
        P("tp"),
        P("sp", "tp"),
        P("sp", "tp"),
    )
    out_specs = (P(("sp", "tp"), None), P("sp", "tp"))
    return jax.shard_map(body, mesh=mesh, in_specs=in_specs, out_specs=out_specs, check_vma=False)
```

profile of v0, /device:TPU:0, one launch (start us, length us, event | category | flops | bytes accessed | tf_op | source)
XLA Modules:
  0.0 450.2 jit_solution(13801407435203110543)
XLA Ops:
  7.3 3.2 convolution_convert_fusion
  18.9 4.7 %slice.626 = f32[191,512]{1,0:T(8,128)} reverse(f32[191,512]{1,0:T(8,128)} %slice.625), dimensions={0} | reverse | bytes 782336 | tf_op jit(solution)/shard_map/slice | solution.py:76
  23.6 4.6 %slice.566 = f32[192,512]{1,0:T(8,128)} reverse(f32[192,512]{1,0:T(8,128)} %slice.565), dimensions={0} | reverse | bytes 786432 | tf_op jit(solution)/shard_map/slice | solution.py:76
  28.2 2.7 slice.568
  37.9 2.8 fusion.80
  40.7 3.2 slice.678
  43.9 3.1 slice.643
  47.0 3.1 slice.642
  56.9 3.2 slice.718
  60.0 3.2 slice.683
  63.2 3.1 slice.682
  94.2 3.1 slice.570
  99.4 3.2 slice.561
  102.6 4.5 %slice.571 = f32[192,512]{1,0:T(8,128)} reverse(f32[192,512]{1,0:T(8,128)} %slice.570), dimensions={0} | reverse | bytes 786432 | tf_op jit(solution)/shard_map/slice | solution.py:76
  107.1 2.7 slice.564
  145.8 2.7 slice.562
  185.5 2.9 pad.213
  223.0 2.9 pad.260
  225.9 3.0 pad.261
  229.6 22.7 %all-gather.2 = f32[16,1,512]{2,1,0:T(1,128)S(1)} all-gather(f32[1,1,512]{2,1,0:T(1,128)S(1)} %add_bitcast_fusion), channel_id=1, replica_groups=mesh['sp'=16,'tp'=2] {'sp'}, dimensions={0}, use_global_device_ids=true | all-gather | bytes 34816 | tf_op jit(solution)/shard_map/all_gather | solution.py:17
  252.3 3.1 pad.245
  256.2 6.9 %rev.8 = f32[384,512]{1,0:T(8,128)} reverse(f32[384,512]{1,0:T(8,128)} %add.495), dimensions={0} | reverse | bytes 1572864 | tf_op jit(solution)/shard_map/rev | solution.py:80
  263.0 17.5 %all-gather.1 = f32[16,1,512]{2,1,0:T(1,128)S(1)} all-gather(f32[1,1,512]{2,1,0:T(1,128)S(1)} %copy-done.61), channel_id=1, replica_groups=mesh['sp'=16,'tp'=2] {'sp'}, dimensions={0}, use_global_device_ids=true | all-gather | bytes 34816 | tf_op jit(solution)/shard_map/all_gather | solution.py:17
  284.2 18.8 %all-gather = f32[16,1,512]{2,1,0:T(1,128)S(1)} all-gather(f32[1,1,512]{2,1,0:T(1,128)S(1)} %add_bitcast_fusion.1), channel_id=1, replica_groups=mesh['sp'=16,'tp'=2] {'sp'}, dimensions={0}, use_global_device_ids=true | all-gather | bytes 34816 | tf_op jit(solution)/shard_map/all_gather | solution.py:17
  303.9 3.3 fusion.78
  308.2 2.9 pad.228
  315.3 6.9 %rev.9 = f32[384,512]{1,0:T(8,128)} reverse(f32[384,512]{1,0:T(8,128)} %add.503), dimensions={0} | reverse | bytes 1572864 | tf_op jit(solution)/shard_map/rev | solution.py:79
  322.3 4.8 %fusion.26 = (bf16[384,512]{1,0:T(8,128)(2,1)}, f32[384,512]{1,0:T(8,128)}, bf16[384,512]{1,0:T(8,128)(2,1)S(1)}) fusion(f32[384,512]{1,0:T(8,128)} %copy.40, f32[384,512]{1,0:T(8,128)} %get-tuple-element.305, f32[384,512]{1,0:T(8,128)} %rev.8, f32[384,512]{1,0:T(8,128)} %rev.9, f32[512]{0:T(512)S(1)} %get-tuple-element.228, f32[384,512]{1,0:T(8,128)} %copy.38, ...), kind=kLoop, calls=%fused_computation.51 | loop fusion | flops 6291456 | bytes 9449472 | tf_op jit(solution)/shard_map/convert_element_type | solution.py:97
  339.2 3.3 convolution_bitcast_fusion
  342.7 2.7 fusion.89
  348.0 67.3 %reduce-scatter.5.cloned.1.call-done = f32[128,512]{0,1:T(8,128)} async-done(((f32[2048,512]{0,1:T(8,128)}), f32[128,512]{0,1:T(8,128)}) %reduce-scatter.5.cloned.1.call-update) | async-done | bytes 262160 | tf_op jit(solution)/shard_map/reduce_scatter | solution.py:126
  417.1 26.3 %reduce-scatter.3.cloned.1.call-done = bf16[192,2048]{1,0:T(8,128)(2,1)} async-done(((bf16[384,2048]{1,0:T(8,128)(2,1)}), bf16[192,2048]{1,0:T(8,128)(2,1)}) %reduce-scatter.3.cloned.1.call-update) | async-done | bytes 786448 | tf_op jit(solution)/shard_map/reduce_scatter | solution.py:137
  (490 shorter events, 187.4 us)
Async XLA Ops:
  7.2 408.1 %reduce-scatter.5.cloned.1.call-start = ((), (), s32[]{:S(2)}) async-start(), calls=%async_computation.3 | async-start | bytes 4456448 | tf_op jit(solution)/shard_map/reduce_scatter | solution.py:126
  10.5 20.4 %collective-permute-start = (bf16[3,512]{1,0:T(4,128)(2,1)S(1)}, bf16[3,512]{1,0:T(4,128)(2,1)S(1)}, u32[]{:S(2)}, u32[]{:S(2)}) collective-permute-start(bf16[3,512]{1,0:T(4,128)(2,1)S(1)} %slice.726), channel_id=1, source_target_pairs={{0,2},{2,4},{4,6},{6,8},{8,10},{10,12},{12,14},{14,16},{16,18},{18... | collective-permute-start | bytes 9224 | tf_op jit(solution)/shard_map/ppermute | solution.py:12
  12.9 40.8 %copy-start.41 = (f32[1,512]{1,0:T(1,128)}, f32[1,512]{1,0:T(1,128)S(1)}, u32[]{:S(2)}) copy-start(f32[1,512]{1,0:T(1,128)S(1)} %get-tuple-element.375) | copy-start | bytes 6148
  13.0 40.8 %copy-start.44 = (f32[1,512]{1,0:T(1,128)}, f32[1,512]{1,0:T(1,128)S(1)}, u32[]{:S(2)}) copy-start(f32[1,512]{1,0:T(1,128)S(1)} %get-tuple-element.376) | copy-start | bytes 6148
  13.0 309.3 %copy-start.37 = (f32[1,512]{1,0:T(1,128)}, f32[1,512]{1,0:T(1,128)S(1)}, u32[]{:S(2)}) copy-start(f32[1,512]{1,0:T(1,128)S(1)} %get-tuple-element.373) | copy-start | bytes 6148
  13.0 309.3 %copy-start.39 = (f32[1,512]{1,0:T(1,128)}, f32[1,512]{1,0:T(1,128)S(1)}, u32[]{:S(2)}) copy-start(f32[1,512]{1,0:T(1,128)S(1)} %get-tuple-element.374) | copy-start | bytes 6148
  14.9 22.9 %copy-start.51 = (f32[512]{0:T(512)}, f32[512]{0:T(512)S(1)}, u32[]{:S(2)}) copy-start(f32[512]{0:T(512)S(1)} %fusion.70) | copy-start | bytes 6148
  37.9 12.3 %copy-start.22 = (bf16[384,512]{0,1:T(8,128)(2,1)S(1)}, bf16[384,512]{0,1:T(8,128)(2,1)}, u32[]{:S(2)}) copy-start(bf16[384,512]{0,1:T(8,128)(2,1)} %copy.36) | copy-start | bytes 1179652
  37.9 12.3 %copy-start.31 = (bf16[8,64,64]{2,1,0:T(8,128)(2,1)S(1)}, bf16[8,64,64]{2,1,0:T(8,128)(2,1)}, u32[]{:S(2)}) copy-start(bf16[8,64,64]{2,1,0:T(8,128)(2,1)} %param.18) | copy-start | bytes 196612
  121.9 24.0 %copy-start.16 = (f32[191,512]{1,0:T(8,128)S(1)}, f32[191,512]{1,0:T(8,128)}, u32[]{:S(2)}) copy-start(f32[191,512]{1,0:T(8,128)} %slice.561) | copy-start | bytes 1173508
  148.6 11.8 %copy-start.25 = (f32[47,512]{1,0:T(8,128)S(1)}, f32[47,512]{1,0:T(8,128)}, u32[]{:S(2)}) copy-start(f32[47,512]{1,0:T(8,128)} %slice.578) | copy-start | bytes 288772
  148.6 11.8 %copy-start.26 = (f32[47,512]{1,0:T(8,128)S(1)}, f32[47,512]{1,0:T(8,128)}, u32[]{:S(2)}) copy-start(f32[47,512]{1,0:T(8,128)} %slice.621) | copy-start | bytes 288772
  185.4 7.1 %copy-start.62 = (f32[1,512]{1,0:T(1,128)S(1)}, f32[1,512]{1,0:T(1,128)}, u32[]{:S(2)}) copy-start(f32[1,512]{1,0:T(1,128)} %slice.811) | copy-start | bytes 6148
  185.5 7.2 %copy-start.33 = (f32[11,512]{1,0:T(8,128)S(1)}, f32[11,512]{1,0:T(8,128)}, u32[]{:S(2)}) copy-start(f32[11,512]{1,0:T(8,128)} %slice.710) | copy-start | bytes 67588
  185.5 7.2 %copy-start.34 = (f32[11,512]{1,0:T(8,128)S(1)}, f32[11,512]{1,0:T(8,128)}, u32[]{:S(2)}) copy-start(f32[11,512]{1,0:T(8,128)} %slice.670) | copy-start | bytes 67588
  192.1 7.6 %copy-start.23 = (f32[47,512]{1,0:T(8,128)S(1)}, f32[47,512]{1,0:T(8,128)}, u32[]{:S(2)}) copy-start(f32[47,512]{1,0:T(8,128)} %slice.714) | copy-start | bytes 288772
  192.1 7.6 %copy-start.24 = (f32[47,512]{1,0:T(8,128)S(1)}, f32[47,512]{1,0:T(8,128)}, u32[]{:S(2)}) copy-start(f32[47,512]{1,0:T(8,128)} %slice.674) | copy-start | bytes 288772
  201.2 8.5 %copy-start.57 = (f32[1,512]{1,0:T(1,128)S(1)}, f32[1,512]{1,0:T(1,128)}, u32[]{:S(2)}) copy-start(f32[1,512]{1,0:T(1,128)} %slice.779) | copy-start | bytes 6148
  202.1 7.6 %copy-start.56 = (f32[1,512]{1,0:T(1,128)S(1)}, f32[1,512]{1,0:T(1,128)}, u32[]{:S(2)}) copy-start(f32[1,512]{1,0:T(1,128)} %slice.807) | copy-start | bytes 6148
  222.2 33.2 %copy-start.14 = (f32[191,512]{1,0:T(8,128)S(1)}, f32[191,512]{1,0:T(8,128)}, u32[]{:S(2)}) copy-start(f32[191,512]{1,0:T(8,128)} %get-tuple-element.313) | copy-start | bytes 1173508
  228.8 34.2 %copy-start.61 = (f32[1,1,512]{2,1,0:T(1,128)S(1)}, f32[1,1,512]{2,1,0:T(1,128)}, u32[]{:S(2)}) copy-start(f32[1,1,512]{2,1,0:T(1,128)} %get-tuple-element.311) | copy-start | bytes 6148
  228.9 51.7 %copy-start.55 = (f32[1,512]{1,0:T(1,128)S(1)}, f32[1,512]{1,0:T(1,128)}, u32[]{:S(2)}) copy-start(f32[1,512]{1,0:T(1,128)} %get-tuple-element.312) | copy-start | bytes 6148
  303.9 7.1 %copy-start.19 = (f32[192,512]{1,0:T(8,128)S(1)}, f32[192,512]{1,0:T(8,128)}, u32[]{:S(2)}) copy-start(f32[192,512]{1,0:T(8,128)} %add.502) | copy-start | bytes 1179652
  312.9 9.3 %copy-start.42 = (f32[1,512]{1,0:T(1,128)S(1)}, f32[1,512]{1,0:T(1,128)}, u32[]{:S(2)}) copy-start(f32[1,512]{1,0:T(1,128)} %copy-done.41) | copy-start | bytes 6148
  313.0 9.3 %copy-start.45 = (f32[1,512]{1,0:T(1,128)S(1)}, f32[1,512]{1,0:T(1,128)}, u32[]{:S(2)}) copy-start(f32[1,512]{1,0:T(1,128)} %copy-done.44) | copy-start | bytes 6148
  313.0 9.3 %copy-start.52 = (f32[512]{0:T(512)S(1)}, f32[512]{0:T(512)}, u32[]{:S(2)}) copy-start(f32[512]{0:T(512)} %copy-done.51) | copy-start | bytes 6148
  331.7 7.1 %copy-start.38 = (f32[1,512]{1,0:T(1,128)S(1)}, f32[1,512]{1,0:T(1,128)}, u32[]{:S(2)}) copy-start(f32[1,512]{1,0:T(1,128)} %copy-done.37) | copy-start | bytes 6148
  331.7 7.1 %copy-start.40 = (f32[1,512]{1,0:T(1,128)S(1)}, f32[1,512]{1,0:T(1,128)}, u32[]{:S(2)}) copy-start(f32[1,512]{1,0:T(1,128)} %copy-done.39) | copy-start | bytes 6148
  331.7 7.1 %copy-start.43 = (f32[1,512]{1,0:T(1,128)S(1)}, f32[1,512]{1,0:T(1,128)}, u32[]{:S(2)}) copy-start(f32[1,512]{1,0:T(1,128)} %copy-done.41) | copy-start | bytes 6148
  331.7 7.1 %copy-start.46 = (f32[1,512]{1,0:T(1,128)S(1)}, f32[1,512]{1,0:T(1,128)}, u32[]{:S(2)}) copy-start(f32[1,512]{1,0:T(1,128)} %copy-done.44) | copy-start | bytes 6148
  335.8 3.1 collective-permute-start.1
  342.6 100.8 %reduce-scatter.3.cloned.1.call-start = ((), (), s32[]{:S(2)}) async-start(), calls=%async_computation.2 | async-start | bytes 2359296 | tf_op jit(solution)/shard_map/reduce_scatter | solution.py:137
  (42 other events, 185.7 us)
Sparse Core Ops, SparseCore 0:
  342.7 72.6 reduce-scatter.4
  418.2 25.1 reduce-scatter.2
where the time goes:
time: 455 us; the launch traced here: 450 us
  local copies, waits for them, and re-layouts  180 us (40%)
  waiting for transfers between devices  95.4 us (21%)
  other arithmetic  75.6 us (17%)
  blocking collectives  59 us (13%)
  matrix products  19.8 us (4%)
  between operations  15.4 us (3%)
    reduce_scatter x1, waiting for transfers between devices, body(): lax.psum_scatter(lax.dot_general(block_input, grad_branch, (((0,), (0,)),...  67.3 us
    slice x61, local copies, waits for them, and re-layouts, body(): lax.associative_scan(combine, (next_decay[::-1], grad_hidden[::-1]), axis=0)  64.1 us
    all_gather x3, blocking collectives, prefix(): everything = jax.tree.map(lambda part: lax.all_gather(part, axis), x)  59 us
    slice x56, local copies, waits for them, and re-layouts, body(): lax.associative_scan(combine, (decays, drive), axis=0)  41.1 us
    reduce_scatter x1, waiting for transfers between devices, body(): lax.psum_scatter((term + lax.dot_general(grad_gate, proj_gate, (((1,), (1...  26.3 us
    pad x30, local copies, waits for them, and re-layouts, body(): lax.associative_scan(combine, (decays, drive), axis=0)  22.5 us
    pad x30, local copies, waits for them, and re-layouts, body(): lax.associative_scan(combine, (next_decay[::-1], grad_hidden[::-1]), axis=0)  20.4 us
    add x15, other arithmetic, body(): lax.associative_scan(combine, (next_decay[::-1], grad_hidden[::-1]), axis=0)  13 us
  transfers between devices with their start and end apart: 4, of which 3 were waited for; matrix products, arithmetic and copies ran while one was open for 6% of the time, Pallas kernels for 0%

commit v1 on v0

v1 whole, which is shorter than its diff:
```python
import functools

import jax
import jax.numpy as jnp
from jax import lax
from jax.experimental import pallas as pl
from jax.experimental.pallas import tpu as pltpu
from jax.sharding import PartitionSpec as P

gate_power = 8.0
LANES = 128
SEGS = 8
HALO = 16
GELU_C = 0.7978845608028654
GELU_K = 0.044715
F32 = jnp.float32
BF16 = jnp.bfloat16
MESH = pl.DeviceIdType.MESH


def neg_expm1(y, ey):
    p = 1.0 + y * (1.0 / 8.0)
    for k in range(7, 1, -1):
        p = 1.0 + y * (1.0 / k) * p
    return jnp.where(y > -0.5, -y * p, 1.0 - ey)


def log_sigmoid(x):
    e = jnp.exp(-jnp.abs(x))
    s = e / (2.0 + e)
    s2 = s * s
    p = jnp.full_like(s, 1.0 / 17.0)
    for k in range(15, 0, -2):
        p = p * s2 + 1.0 / k
    return jnp.minimum(x, 0.0) - 2.0 * s * p


def dot(a, b, dims=((1,), (0,))):
    return lax.dot_general(a, b, (dims, ((), ())), preferred_element_type=F32)


def factor(n):
    bits, last = 0, n
    while last > 4 and last % 2 == 0:
        last //= 2
        bits += 1
    return last, bits


def bitrev(v, bits):
    out = 0
    for i in range(bits):
        out = out * 2 + (v >> i) % 2
    return out


def kernel(
    n_sp, n_tp, x_hbm, wx_hbm, wg_hbm, taps, ga, gi, dp, lj_hbm, og_hbm,
    gin_out, gproj_out,
    xs, wx, wg, lj, og, gt, br, mix, mixb, bda, bdi, rec, ing, dec, nrm, us, ps, gs, qs,
    cs, rs, sbuf, rbuf, pab, pib, gg, gm, gb, acc, tsend, trecv, part, srecv, sacc, lrecv,
    loc_sem, halo_sem, msend_sem, mrecv_sem, head_sem, tsend_sem, trecv_sem, ssend_sem,
    srecv_sem, lsend_sem, lrecv_sem,
):
    me = lax.axis_index("sp")
    tp = lax.axis_index("tp")
    rows, chans = og.shape
    depth = wx.shape[0]
    nq = chans // LANES
    taps_n = taps.shape[0]
    block = ga.shape[1]
    seg = rows // SEGS
    last, bits = factor(n_sp)
    per_last = n_sp // last

    barrier = pltpu.get_barrier_semaphore()
    for k in range(1, n_sp):
        pl.semaphore_signal(
            barrier, inc=1, device_id={"sp": lax.rem(me + k, n_sp)}, device_id_type=MESH
        )
    for k in range(1, n_tp):
        pl.semaphore_signal(
            barrier, inc=1, device_id={"tp": lax.rem(tp + k, n_tp)}, device_id_type=MESH
        )
    loads = []
    for i, (src, dst) in enumerate(
        ((x_hbm, xs.at[pl.ds(HALO, rows)]), (wg_hbm, wg), (wx_hbm, wx), (lj_hbm, lj), (og_hbm, og))
    ):
        c = pltpu.make_async_copy(src, dst, loc_sem.at[i])
        c.start()
        loads.append(c)

    gw = bda.shape[1]
    spread = (
        lax.rem(lax.broadcasted_iota(jnp.int32, (block, gw), 1), block)
        == lax.broadcasted_iota(jnp.int32, (block, gw), 0)
    ).astype(F32).astype(BF16)
    keep = lax.rem(lax.broadcasted_iota(jnp.int32, (chans, gw), 0), gw) // block == (
        lax.broadcasted_iota(jnp.int32, (chans, gw), 1) // block
    )
    for src, dst in ((ga, bda), (gi, bdi)):
        flat = src[...].reshape(chans, block)
        dst[...] = jnp.where(keep, dot(flat, spread), 0.0).astype(BF16)

    loads[0].wait()
    pl.semaphore_wait(barrier, n_sp - 1 + n_tp - 1)
    halo = pltpu.make_async_remote_copy(
        src_ref=xs.at[pl.ds(rows, HALO)], dst_ref=xs.at[pl.ds(0, HALO)],
        send_sem=halo_sem.at[0], recv_sem=halo_sem.at[1],
        device_id={"sp": lax.rem(me + 1, n_sp)}, device_id_type=MESH,
    )
    halo.start()
    loads[1].wait()
    pre = dot(xs[pl.ds(HALO, rows), :], wg[...]).astype(BF16).astype(F32)
    for q in range(nq):
        gt[q] = pre[:, q * LANES : (q + 1) * LANES]
    loads[2].wait()
    halo.wait_recv()
    pre = dot(xs[...], wx[...]).astype(BF16).astype(F32)
    for q in range(nq):
        br[q] = pre[:, q * LANES : (q + 1) * LANES]
    first = me == 0
    for q in range(nq):
        br[q, pl.ds(0, HALO), :] = jnp.where(first, 0.0, br[q, pl.ds(0, HALO), :])

    step = 128 if rows % 128 == 0 else rows
    for q in range(nq):
        lanes = slice(q * LANES, (q + 1) * LANES)
        for r in range(0, rows, step):
            total = jnp.zeros((step, LANES), F32)
            for j in range(taps_n):
                off = HALO - taps_n + 1 + j + r
                total = total + taps[j : j + 1, lanes] * br[q, off : off + step, :]
            half = total.astype(BF16)
            mixb[r : r + step, lanes] = half
            mix[q, r : r + step, :] = half.astype(F32)

    for src, dst in ((bda, rec), (bdi, ing)):
        for g in range(chans // gw):
            cols = slice(g * gw, (g + 1) * gw)
            pre = dot(mixb[:, cols], src[cols, :])
            for q in range(gw // LANES):
                dst[g * (gw // LANES) + q] = pre[:, q * LANES : (q + 1) * LANES]

    loads[3].wait()
    loads[4].wait()
    sub = 64 if rows % 64 == 0 else rows
    log_sig = log_sigmoid(dp[...])
    for q in range(nq):
        lanes = slice(q * LANES, (q + 1) * LANES)
        scale = gate_power * log_sig[:, lanes]

        def gates(i, carry, q=q, lanes=lanes, scale=scale):
            r = pl.ds(pl.multiple_of(i * sub, sub), sub)
            rg = jax.nn.sigmoid(rec[q, r, :])
            ig = jax.nn.sigmoid(ing[q, r, :])
            log_decay = rg * scale + lj[r, lanes]
            a = jnp.exp(log_decay)
            v = neg_expm1(2.0 * log_decay, a * a)
            norm = jnp.sqrt(v)
            rec[q, r, :] = rg
            ing[q, r, :] = ig
            dec[q, r, :] = a
            nrm[q, r, :] = norm
            us[q, r, :] = norm * ig * mix[q, r, :]
            z = gt[q, r, :]
            t = jnp.tanh(GELU_C * (z + GELU_K * (z * z * z)))
            gs[q, r, :] = og[r, lanes].astype(F32) * (0.5 * z * (1.0 + t))
            return carry

        lax.fori_loop(0, rows // sub, gates, 0)

    def scan(i, carry):
        out = []
        for q in range(nq):
            h, p, g, w = carry[q]
            f = pl.ds(i, SEGS, stride=seg)
            b = pl.ds(seg - 1 - i, SEGS, stride=seg)
            a = dec[q, f, :]
            u = a * h
            h = u + us[q, f, :]
            p = a * p
            us[q, f, :] = u
            ps[q, f, :] = p
            g = gs[q, b, :] + g
            gs[q, b, :] = g
            qs[q, b, :] = w
            a = dec[q, b, :]
            out.append((h, p, a * g, a * w))
        return tuple(out)

    zero = jnp.zeros((SEGS, LANES), F32)
    one = jnp.ones((SEGS, LANES), F32)
    ends = lax.fori_loop(0, seg, scan, tuple((zero, one, zero, one) for _ in range(nq)), unroll=2)
    for q in range(nq):
        h, p, g, _ = ends[q]
        fwd = jnp.zeros((1, LANES), F32)
        bwd = jnp.zeros((1, LANES), F32)
        prod = jnp.ones((1, LANES), F32)
        for s in range(SEGS):
            e = SEGS - 1 - s
            fwd = p[s : s + 1] * fwd + h[s : s + 1]
            bwd = p[e : e + 1] * bwd + g[e : e + 1]
            prod = prod * p[s : s + 1]
        sbuf[0, q : q + 1, :] = prod
        sbuf[1, q : q + 1, :] = prod
        sbuf[0, nq + q : nq + q + 1, :] = fwd
        sbuf[1, nq + q : nq + q + 1, :] = bwd

    sent = []
    for k in range(1, n_sp):
        peer = lax.rem(me + k, n_sp)
        c = pltpu.make_async_remote_copy(
            src_ref=sbuf.at[jnp.where(peer > me, 0, 1)], dst_ref=rbuf.at[k],
            send_sem=msend_sem.at[k], recv_sem=mrecv_sem.at[k],
            device_id={"sp": peer}, device_id_type=MESH,
        )
        c.start()
        sent.append(c)
    for c in sent:
        c.wait_recv()
    fwd = jnp.zeros((nq, LANES), F32)
    bwd = jnp.zeros((nq, LANES), F32)
    for k in range(n_sp - 1, 0, -1):
        fwd = jnp.where(me >= k, rbuf[k, 0:nq, :] * fwd + rbuf[k, nq : 2 * nq, :], fwd)
    for k in range(1, n_sp):
        bwd = jnp.where(me < k, rbuf[k, 0:nq, :] * bwd + rbuf[k, nq : 2 * nq, :], bwd)
    for q in range(nq):
        h, p, g, _ = ends[q]
        c = fwd[q : q + 1]
        d = bwd[q : q + 1]
        for s in range(SEGS):
            e = SEGS - 1 - s
            cs[q, s : s + 1, :] = c
            rs[q, e : e + 1, :] = d
            c = p[s : s + 1] * c + h[s : s + 1]
            d = p[e : e + 1] * d + g[e : e + 1]

    for q in range(nq):
        lanes = slice(q * LANES, (q + 1) * LANES)
        scale = gate_power * log_sig[:, lanes]

        def grads(s, carry, q=q, lanes=lanes, scale=scale):
            r = pl.ds(pl.multiple_of(s * seg, seg), seg)
            a = dec[q, r, :]
            norm = nrm[q, r, :]
            ig = ing[q, r, :]
            rg = rec[q, r, :]
            m = mix[q, r, :]
            u = us[q, r, :] + ps[q, r, :] * cs[q, pl.ds(s, 1), :]
            state = gs[q, r, :] + qs[q, r, :] * rs[q, pl.ds(s, 1), :]
            im = ig * m
            hid = (u + norm * im).astype(BF16).astype(F32)
            grad_log = state * (u - im * (a * a) / norm)
            pab[r, lanes] = (grad_log * scale * (rg * (1.0 - rg))).astype(BF16)
            sn = state * norm
            pib[r, lanes] = (sn * im * (1.0 - ig)).astype(BF16)
            gm[q, r, :] = sn * ig
            z = gt[q, r, :]
            z2 = z * z
            t = jnp.tanh(GELU_C * (z + GELU_K * (z2 * z)))
            slope = 0.5 * (1.0 + t) + (0.5 * GELU_C) * z * (1.0 - t * t) * (
                1.0 + (3.0 * GELU_K) * z2
            )
            gg[r, lanes] = (og[r, lanes].astype(F32) * hid * slope).astype(BF16)
            return carry

        lax.fori_loop(0, SEGS, grads, 0)

    for g in range(chans // gw):
        cols = slice(g * gw, (g + 1) * gw)
        back = dot(pab[:, cols], bda[cols, :], ((1,), (1,)))
        back = back + dot(pib[:, cols], bdi[cols, :], ((1,), (1,)))
        for q in range(gw // LANES):
            at = g * (gw // LANES) + q
            gm[at, 0:rows, :] = gm[at, 0:rows, :] + back[:, q * LANES : (q + 1) * LANES]
    head = pltpu.make_async_remote_copy(
        src_ref=gm.at[:, pl.ds(0, 8), :], dst_ref=gm.at[:, pl.ds(rows, 8), :],
        send_sem=head_sem.at[0], recv_sem=head_sem.at[1],
        device_id={"sp": lax.rem(me + n_sp - 1, n_sp)}, device_id_type=MESH,
    )
    head.start()
    width = 512 if depth % 512 == 0 else depth
    for d in range(0, depth, width):
        acc[:, d : d + width] = dot(gg[...], wg[d : d + width, :], ((1,), (1,)))
    head.wait_recv()
    final = me == n_sp - 1
    for q in range(nq):
        gm[q, rows : rows + 8, :] = jnp.where(final, 0.0, gm[q, rows : rows + 8, :])
    for q in range(nq):
        lanes = slice(q * LANES, (q + 1) * LANES)
        for r in range(0, rows, step):
            total = jnp.zeros((step, LANES), F32)
            for j in range(taps_n):
                off = taps_n - 1 - j + r
                total = total + taps[j : j + 1, lanes] * gm[q, off : off + step, :]
            gb[r : r + step, lanes] = total.astype(BF16)

    order = list(range(1, last)) + [0]
    wide = depth // last
    share = depth // n_sp
    zi = me // per_last
    inner = lax.rem(me, per_last)

    def digit(i):
        return lax.rem(inner // (2**i), 2)

    def partner(i):
        return me + (1 - 2 * digit(i)) * (2**i)

    def stage_copy(i, k):
        size = 2 ** (bits - 1 - i)
        off = (1 - digit(i)) * size
        src = part.at[k, pl.ds(off, size)] if i == 0 else sacc.at[i - 1, k, pl.ds(off, size)]
        return pltpu.make_async_remote_copy(
            src_ref=src, dst_ref=srecv.at[i, k, pl.ds(0, size)],
            send_sem=ssend_sem.at[i, k], recv_sem=srecv_sem.at[i, k],
            device_id={"sp": partner(i)}, device_id_type=MESH,
        )

    def last_copy(k):
        src = part.at[k, 0] if bits == 0 else sacc.at[bits - 1, k, 0]
        return pltpu.make_async_remote_copy(
            src_ref=src, dst_ref=lrecv.at[k],
            send_sem=lsend_sem.at[k], recv_sem=lrecv_sem.at[k],
            device_id={"sp": lax.rem(zi + k, last) * per_last + inner}, device_id_type=MESH,
        )

    own = rows // n_tp
    pieces = tsend.shape[1]
    piece = depth // pieces

    def term(at, c):
        r = pl.ds(pl.multiple_of(at * own, own), own)
        cols = slice(c * piece, (c + 1) * piece)
        return acc[r, cols] + dot(gb[r, :], wx[cols, :], ((1,), (1,)))

    def term_copy(k, c):
        return pltpu.make_async_remote_copy(
            src_ref=tsend.at[k - 1, c], dst_ref=trecv.at[k - 1, c],
            send_sem=tsend_sem.at[k - 1, c], recv_sem=trecv_sem.at[k - 1, c],
            device_id={"tp": lax.rem(tp + k, n_tp)}, device_id_type=MESH,
        )

    def product(k):
        zd = lax.rem(zi + k, last)
        at = pl.ds(pl.multiple_of(zd * wide, wide), wide)
        prod = dot(xs[pl.ds(HALO, rows), at], gb[...], ((0,), (0,)))
        for v in range(per_last):
            part[k, bitrev(v, bits)] = prod[v * share : (v + 1) * share].astype(BF16)
        if bits:
            stage_copy(0, k).start()
        elif k:
            last_copy(k).start()

    def terms(c):
        for k in range(1, n_tp):
            tsend[k - 1, c] = term(lax.rem(tp + k, n_tp), c).astype(BF16)
            term_copy(k, c).start()

    terms(0)
    for k in order[:2]:
        product(k)
    for c in range(1, pieces):
        terms(c)
    for k in order[2:]:
        product(k)
    for i in range(bits):
        size = 2 ** (bits - 1 - i)
        for k in order:
            stage_copy(i, k).wait_recv()
            off = digit(i) * size
            for v in range(size):
                mine = part[k, off + v] if i == 0 else sacc[i - 1, k, off + v]
                sacc[i, k, v] = (mine.astype(F32) + srecv[i, k, v].astype(F32)).astype(BF16)
            if i + 1 < bits:
                stage_copy(i + 1, k).start()
            elif k:
                last_copy(k).start()
    for c in range(pieces):
        tsend[n_tp - 1, c] = term(tp, c).astype(BF16)
    total = (part[0, 0] if bits == 0 else sacc[bits - 1, 0, 0]).astype(F32)
    for k in range(1, last):
        last_copy(k).wait_recv()
        total = total + lrecv[k].astype(F32)
    gproj_out[...] = total
    for c in range(pieces):
        cols = slice(c * piece, (c + 1) * piece)
        total = tsend[n_tp - 1, c].astype(F32)
        for k in range(1, n_tp):
            term_copy(k, c).wait_recv()
            total = total + trecv[k - 1, c].astype(F32)
        gin_out[:, cols] = total.astype(BF16)

    halo.wait_send()
    head.wait_send()
    for c in sent:
        c.wait_send()
    for i in range(bits):
        for k in order:
            stage_copy(i, k).wait_send()
    for k in range(1, last):
        last_copy(k).wait_send()
    for c in range(pieces):
        for k in range(1, n_tp):
            term_copy(k, c).wait_send()


def body(n_sp, n_tp, block_input, proj_x, proj_gate, conv_taps, gate_a, gate_in, decay_param,
         log_jump, out_grad):
    rows, depth = block_input.shape
    chans = proj_x.shape[1]
    nq = chans // LANES
    gw = 256 if chans % 256 == 0 else LANES
    last, bits = factor(n_sp)
    per_last = n_sp // last
    share = depth // n_sp
    own = rows // n_tp
    pieces = 2
    stages = max(bits, 1)
    most = max(per_last // 2, 1)
    vm = pltpu.VMEM
    grid_f32 = vm((nq, rows, LANES), F32)
    dma = pltpu.SemaphoreType.DMA
    anywhere = pl.BlockSpec(memory_space=pl.ANY)
    local = pl.BlockSpec(memory_space=pltpu.VMEM)
    scratch = [
        vm((rows + HALO, depth), BF16), vm((depth, chans), BF16), vm((depth, chans), BF16),
        vm((rows, chans), F32), vm((rows, chans), BF16),
        grid_f32, vm((nq, rows + HALO, LANES), F32), grid_f32, vm((rows, chans), BF16),
        vm((chans, gw), BF16), vm((chans, gw), BF16),
        grid_f32, grid_f32, grid_f32, grid_f32, grid_f32, grid_f32, grid_f32, grid_f32,
        vm((nq, SEGS, LANES), F32), vm((nq, SEGS, LANES), F32),
        vm((2, 2 * nq, LANES), F32), vm((n_sp, 2 * nq, LANES), F32),
        vm((rows, chans), BF16), vm((rows, chans), BF16), vm((rows, chans), BF16),
        vm((nq, rows + 8, LANES), F32), vm((rows, chans), BF16), vm((rows, depth), F32),
        vm((n_tp, pieces, own, depth // pieces), BF16),
        vm((max(n_tp - 1, 1), pieces, own, depth // pieces), BF16),
        vm((last, per_last, share, chans), BF16),
        vm((stages, last, most, share, chans), BF16),
        vm((stages, last, most, share, chans), BF16),
        vm((last, share, chans), BF16),
        dma((5,)), dma((2,)), dma((n_sp,)), dma((n_sp,)), dma((2,)),
        dma((n_tp, pieces)), dma((n_tp, pieces)), dma((stages, last)), dma((stages, last)),
        dma((last,)), dma((last,)),
    ]
    return pl.pallas_call(
        functools.partial(kernel, n_sp, n_tp),
        out_shape=(
            jax.ShapeDtypeStruct((own, depth), BF16),
            jax.ShapeDtypeStruct((share, chans), F32),
        ),
        in_specs=[anywhere] * 3 + [local] * 4 + [anywhere] * 2,
        out_specs=(local, local),
        scratch_shapes=scratch,
        compiler_params=pltpu.CompilerParams(
            collective_id=0, has_side_effects=True, vmem_limit_bytes=56 * 1024 * 1024
        ),
    )(block_input, proj_x, proj_gate, conv_taps, gate_a, gate_in, decay_param.reshape(1, chans),
      log_jump, out_grad)


def solution(mesh):
    in_specs = (
        P("sp", None),
        P(None, "tp"),
        P(None, "tp"),
        P(None, "tp"),
        P("tp", None, None),
        P("tp", None, None),
        P("tp"),
        P("sp", "tp"),
        P("sp", "tp"),
    )
    out_specs = (P(("sp", "tp"), None), P("sp", "tp"))
    return jax.shard_map(
        functools.partial(body, mesh.shape["sp"], mesh.shape["tp"]),
        mesh=mesh, in_specs=in_specs, out_specs=out_specs, check_vma=False,
    )
```

time: 455 us -> 51.2 us (0.11)
  local copies, waits for them, and re-layouts: 180 us -> 3.76 us
  waiting for transfers between devices: 95.4 us -> 0 us
  other arithmetic: 75.6 us -> 0 us
  blocking collectives: 59 us -> 0 us
  Pallas kernels: 0 us -> 46.6 us
  matrix products: 19.8 us -> 0 us
  between operations: 15.4 us -> 0.64 us
    slice x121 -> x0, local copies, waits for them, and re-layouts: 106 us -> none  [the longest x61 64.1 us: body(): lax.associative_scan(combine, (next_decay[::-1], grad_hidden[::-1]), axis=0)]
    reduce_scatter x2 -> x0, waiting for transfers between devices: 93.6 us -> none  [the longest x1 67.3 us: body(): lax.psum_scatter(lax.dot_general(block_input, grad_branch, (((0,), (0,)),...]
    all_gather x3 -> x0, blocking collectives: 59 us -> none  [prefix(): everything = jax.tree.map(lambda part: lax.all_gather(part, axis), x)]
    pallas_call x0 -> x1, Pallas kernels: none -> 46.6 us  [body(): pl.pallas_call(functools.partial(kernel, n_sp, n_tp), out_shape=(jax.Shap...]
    pad x60 -> x0, local copies, waits for them, and re-layouts: 42.9 us -> none  [the longest x30 22.5 us: body(): lax.associative_scan(combine, (decays, drive), axis=0)]
    add x44 -> x0, other arithmetic: 30.1 us -> none  [the longest x15 13 us: body(): lax.associative_scan(combine, (next_decay[::-1], grad_hidden[::-1]), axis=0)]
    dot_general x9 -> x0, matrix products: 19.8 us -> none  [the longest x1 3.32 us: body(): lax.dot_general(block_input, grad_branch, (((0,), (0,)), ((), ())), prefe...]
    concatenate x29 -> x0, other arithmetic: 15.2 us -> none  [the longest x14 8.03 us: body(): lax.associative_scan(combine, (next_decay[::-1], grad_hidden[::-1]), axis=0)]
  transfers between devices with their start and end apart: 4 -> 0, of which waited for: 3 -> 0; matrix products, arithmetic and copies ran while one was open for 6% -> 0% of each run, Pallas kernels for 0% -> 0%
where the time goes in v1:
time: 51.2 us; the launch traced here: 51 us
  Pallas kernels  46.6 us (91%)
  local copies, waits for them, and re-layouts  3.76 us (7%)
  between operations  0.64 us (1%)
    pallas_call x1, Pallas kernels, body(): pl.pallas_call(functools.partial(kernel, n_sp, n_tp), out_shape=(jax.Shap...  46.6 us
    unnamed x2, local copies, waits for them, and re-layouts  3.76 us

profile of v1, /device:TPU:0, one launch (start us, length us, event | category | flops | bytes accessed | tf_op | source)
XLA Modules:
  0.0 51.0 jit_solution(16568571767847882384)
XLA Ops:
  0.6 46.6 %shard_map.104 = (bf16[192,2048]{1,0:T(8,128)(2,1)}, f32[128,512]{1,0:T(8,128)}) custom-call(bf16[384,2048]{1,0:T(8,128)(2,1)} %x_hbm.1, bf16[2048,512]{1,0:T(8,128)(2,1)} %wx_hbm.1, bf16[2048,512]{1,0:T(8,128)(2,1)} %wg_hbm.1, f32[4,512]{1,0:T(4,128)} %taps.1, bf16[8,64,64]{2,1,0:T(8,128)(2,1)} %ga.1, bf16[8,64,64]{2,1,0:T(8,128)(2,1)} %gi.1, ...), custom_call_target="tpu_custom_call" | custom-call | tf_op jit(solution)/shard_map/pallas_call | solution.py:447
  47.2 2.1 %copy.13 = bf16[192,2048]{1,0:T(8,128)(2,1)} copy(bf16[192,2048]{1,0:T(8,128)(2,1)} %get-tuple-element.4) | data formatting | bytes 1572864
  49.3 1.7 %copy.14 = f32[128,512]{1,0:T(8,128)} copy(f32[128,512]{1,0:T(8,128)} %get-tuple-element.5) | data formatting | bytes 524288

commit v2 on v1

--- a/solution.py
+++ b/solution.py
@@ -55,9 +55,9 @@
 
 
 def kernel(
-    n_sp, n_tp, x_hbm, wx_hbm, wg_hbm, taps, ga, gi, dp, lj_hbm, og_hbm,
+    n_sp, n_tp, x_hbm, wx_hbm, wg_hbm, taps_hbm, ga_hbm, gi_hbm, dp_hbm, lj_hbm, og_hbm,
     gin_out, gproj_out,
-    xs, wx, wg, lj, og, gt, br, mix, mixb, bda, bdi, rec, ing, dec, nrm, us, ps, gs, qs,
+    taps, ga, gi, dp, xs, wx, wg, lj, og, gt, br, mix, mixb, bda, bdi, rec, ing, dec, nrm, us, ps, gs, qs,
     cs, rs, sbuf, rbuf, pab, pib, gg, gm, gb, acc, tsend, trecv, part, srecv, sacc, lrecv,
     loc_sem, halo_sem, msend_sem, mrecv_sem, head_sem, tsend_sem, trecv_sem, ssend_sem,
     srecv_sem, lsend_sem, lrecv_sem,
@@ -84,7 +84,8 @@
         )
     loads = []
     for i, (src, dst) in enumerate(
-        ((x_hbm, xs.at[pl.ds(HALO, rows)]), (wg_hbm, wg), (wx_hbm, wx), (lj_hbm, lj), (og_hbm, og))
+        ((x_hbm, xs), (wg_hbm, wg), (wx_hbm, wx), (lj_hbm, lj), (og_hbm, og),
+         (ga_hbm, ga), (gi_hbm, gi), (dp_hbm, dp), (taps_hbm, taps))
     ):
         c = pltpu.make_async_copy(src, dst, loc_sem.at[i])
         c.start()
@@ -98,35 +99,34 @@
     keep = lax.rem(lax.broadcasted_iota(jnp.int32, (chans, gw), 0), gw) // block == (
         lax.broadcasted_iota(jnp.int32, (chans, gw), 1) // block
     )
-    for src, dst in ((ga, bda), (gi, bdi)):
-        flat = src[...].reshape(chans, block)
-        dst[...] = jnp.where(keep, dot(flat, spread), 0.0).astype(BF16)
 
     loads[0].wait()
+    loads[1].wait()
+    pre = dot(xs[...], wg[...]).astype(BF16).astype(F32)
+    for q in range(nq):
+        gt[q] = pre[:, q * LANES : (q + 1) * LANES]
+    loads[2].wait()
+    pre = dot(xs[...], wx[...]).astype(BF16).astype(F32)
+    for q in range(nq):
+        br[q, HALO:, :] = pre[:, q * LANES : (q + 1) * LANES]
+    for load in loads[3:]:
+        load.wait()
     pl.semaphore_wait(barrier, n_sp - 1 + n_tp - 1)
     halo = pltpu.make_async_remote_copy(
-        src_ref=xs.at[pl.ds(rows, HALO)], dst_ref=xs.at[pl.ds(0, HALO)],
+        src_ref=br.at[:, pl.ds(rows + HALO - 8, 8), :], dst_ref=br.at[:, pl.ds(HALO - 8, 8), :],
         send_sem=halo_sem.at[0], recv_sem=halo_sem.at[1],
         device_id={"sp": lax.rem(me + 1, n_sp)}, device_id_type=MESH,
     )
     halo.start()
-    loads[1].wait()
-    pre = dot(xs[pl.ds(HALO, rows), :], wg[...]).astype(BF16).astype(F32)
-    for q in range(nq):
-        gt[q] = pre[:, q * LANES : (q + 1) * LANES]
-    loads[2].wait()
-    halo.wait_recv()
-    pre = dot(xs[...], wx[...]).astype(BF16).astype(F32)
-    for q in range(nq):
-        br[q] = pre[:, q * LANES : (q + 1) * LANES]
-    first = me == 0
-    for q in range(nq):
-        br[q, pl.ds(0, HALO), :] = jnp.where(first, 0.0, br[q, pl.ds(0, HALO), :])
-
-    step = 128 if rows % 128 == 0 else rows
-    for q in range(nq):
-        lanes = slice(q * LANES, (q + 1) * LANES)
-        for r in range(0, rows, step):
+    for src, dst in ((ga, bda), (gi, bdi)):
+        flat = src[...].reshape(chans, block)
+        dst[...] = jnp.where(keep, dot(flat, spread), 0.0).astype(BF16)
+
+    log_sig = log_sigmoid(dp[...])
+
+    def convolve(r, step):
+        for q in range(nq):
+            lanes = slice(q * LANES, (q + 1) * LANES)
             total = jnp.zeros((step, LANES), F32)
             for j in range(taps_n):
                 off = HALO - taps_n + 1 + j + r
@@ -135,40 +135,57 @@
             mixb[r : r + step, lanes] = half
             mix[q, r : r + step, :] = half.astype(F32)
 
-    for src, dst in ((bda, rec), (bdi, ing)):
-        for g in range(chans // gw):
-            cols = slice(g * gw, (g + 1) * gw)
-            pre = dot(mixb[:, cols], src[cols, :])
-            for q in range(gw // LANES):
-                dst[g * (gw // LANES) + q] = pre[:, q * LANES : (q + 1) * LANES]
-
-    loads[3].wait()
-    loads[4].wait()
+    def gate_maps(r, count):
+        for src, dst in ((bda, rec), (bdi, ing)):
+            for g in range(chans // gw):
+                cols = slice(g * gw, (g + 1) * gw)
+                pre = dot(mixb[r : r + count, cols], src[cols, :])
+                for q in range(gw // LANES):
+                    dst[g * (gw // LANES) + q, r : r + count, :] = (
+                        pre[:, q * LANES : (q + 1) * LANES]
+                    )
+
+    def gates(q, r):
+        lanes = slice(q * LANES, (q + 1) * LANES)
+        rg = jax.nn.sigmoid(rec[q, r, :])
+        ig = jax.nn.sigmoid(ing[q, r, :])
+        log_decay = rg * (gate_power * log_sig[:, lanes]) + lj[r, lanes]
+        a = jnp.exp(log_decay)
+        norm = jnp.sqrt(neg_expm1(2.0 * log_decay, a * a))
+        rec[q, r, :] = rg
+        ing[q, r, :] = ig
+        dec[q, r, :] = a
+        nrm[q, r, :] = norm
+        us[q, r, :] = norm * ig * mix[q, r, :]
+
     sub = 64 if rows % 64 == 0 else rows
-    log_sig = log_sigmoid(dp[...])
-    for q in range(nq):
-        lanes = slice(q * LANES, (q + 1) * LANES)
-        scale = gate_power * log_sig[:, lanes]
-
-        def gates(i, carry, q=q, lanes=lanes, scale=scale):
+    step = 128 if rows % 128 == 0 else rows
+    for q in range(nq):
+        mix[q, 0:HALO, :] = jnp.zeros((HALO, LANES), F32)
+        rec[q, 0:HALO, :] = jnp.zeros((HALO, LANES), F32)
+        ing[q, 0:HALO, :] = jnp.zeros((HALO, LANES), F32)
+    for r in range(HALO, rows, step):
+        convolve(r, min(step, rows - r))
+    gate_maps(HALO, rows - HALO)
+    for q in range(nq):
+
+        def most(i, carry, q=q):
             r = pl.ds(pl.multiple_of(i * sub, sub), sub)
-            rg = jax.nn.sigmoid(rec[q, r, :])
-            ig = jax.nn.sigmoid(ing[q, r, :])
-            log_decay = rg * scale + lj[r, lanes]
-            a = jnp.exp(log_decay)
-            v = neg_expm1(2.0 * log_decay, a * a)
-            norm = jnp.sqrt(v)
-            rec[q, r, :] = rg
-            ing[q, r, :] = ig
-            dec[q, r, :] = a
-            nrm[q, r, :] = norm
-            us[q, r, :] = norm * ig * mix[q, r, :]
+            gates(q, r)
             z = gt[q, r, :]
             t = jnp.tanh(GELU_C * (z + GELU_K * (z * z * z)))
-            gs[q, r, :] = og[r, lanes].astype(F32) * (0.5 * z * (1.0 + t))
+            gs[q, r, :] = og[r, q * LANES : (q + 1) * LANES].astype(F32) * (0.5 * z * (1.0 + t))
             return carry
 
-        lax.fori_loop(0, rows // sub, gates, 0)
+        lax.fori_loop(0, rows // sub, most, 0)
+    halo.wait_recv()
+    first = me == 0
+    for q in range(nq):
+        br[q, HALO - 8 : HALO, :] = jnp.where(first, 0.0, br[q, HALO - 8 : HALO, :])
+    convolve(0, HALO)
+    gate_maps(0, HALO)
+    for q in range(nq):
+        gates(q, pl.ds(0, HALO))
 
     def scan(i, carry):
         out = []
@@ -217,6 +234,32 @@
         )
         c.start()
         sent.append(c)
+    for q in range(nq):
+
+        def ready(i, carry, q=q):
+            r = pl.ds(pl.multiple_of(i * sub, sub), sub)
+            lanes = slice(q * LANES, (q + 1) * LANES)
+            a = dec[q, r, :]
+            norm = nrm[q, r, :]
+            ig = ing[q, r, :]
+            rg = rec[q, r, :]
+            im = ig * mix[q, r, :]
+            drive = norm * im
+            mix[q, r, :] = drive
+            dec[q, r, :] = im * (a * a) / norm
+            rec[q, r, :] = (gate_power * log_sig[:, lanes]) * (rg * (1.0 - rg))
+            nrm[q, r, :] = drive * (1.0 - ig)
+            ing[q, r, :] = norm * ig
+            z = gt[q, r, :]
+            z2 = z * z
+            t = jnp.tanh(GELU_C * (z + GELU_K * (z2 * z)))
+            slope = 0.5 * (1.0 + t) + (0.5 * GELU_C) * z * (1.0 - t * t) * (
+                1.0 + (3.0 * GELU_K) * z2
+            )
+            gt[q, r, :] = og[r, lanes].astype(F32) * slope
+            return carry
+
+        lax.fori_loop(0, rows // sub, ready, 0)
     for c in sent:
         c.wait_recv()
     fwd = jnp.zeros((nq, LANES), F32)
@@ -236,50 +279,45 @@
             c = p[s : s + 1] * c + h[s : s + 1]
             d = p[e : e + 1] * d + g[e : e + 1]
 
-    for q in range(nq):
+    def grads(q, s):
+        r = pl.ds(s * seg if isinstance(s, int) else pl.multiple_of(s * seg, seg), seg)
         lanes = slice(q * LANES, (q + 1) * LANES)
-        scale = gate_power * log_sig[:, lanes]
-
-        def grads(s, carry, q=q, lanes=lanes, scale=scale):
-            r = pl.ds(pl.multiple_of(s * seg, seg), seg)
-            a = dec[q, r, :]
-            norm = nrm[q, r, :]
-            ig = ing[q, r, :]
-            rg = rec[q, r, :]
-            m = mix[q, r, :]
-            u = us[q, r, :] + ps[q, r, :] * cs[q, pl.ds(s, 1), :]
-            state = gs[q, r, :] + qs[q, r, :] * rs[q, pl.ds(s, 1), :]
-            im = ig * m
-            hid = (u + norm * im).astype(BF16).astype(F32)
-            grad_log = state * (u - im * (a * a) / norm)
-            pab[r, lanes] = (grad_log * scale * (rg * (1.0 - rg))).astype(BF16)
-            sn = state * norm
-            pib[r, lanes] = (sn * im * (1.0 - ig)).astype(BF16)
-            gm[q, r, :] = sn * ig
-            z = gt[q, r, :]
-            z2 = z * z
-            t = jnp.tanh(GELU_C * (z + GELU_K * (z2 * z)))
-            slope = 0.5 * (1.0 + t) + (0.5 * GELU_C) * z * (1.0 - t * t) * (
-                1.0 + (3.0 * GELU_K) * z2
-            )
-            gg[r, lanes] = (og[r, lanes].astype(F32) * hid * slope).astype(BF16)
-            return carry
-
-        lax.fori_loop(0, SEGS, grads, 0)
-
-    for g in range(chans // gw):
-        cols = slice(g * gw, (g + 1) * gw)
-        back = dot(pab[:, cols], bda[cols, :], ((1,), (1,)))
-        back = back + dot(pib[:, cols], bdi[cols, :], ((1,), (1,)))
-        for q in range(gw // LANES):
-            at = g * (gw // LANES) + q
-            gm[at, 0:rows, :] = gm[at, 0:rows, :] + back[:, q * LANES : (q + 1) * LANES]
+        u = us[q, r, :] + ps[q, r, :] * cs[q, pl.ds(s, 1), :]
+        state = gs[q, r, :] + qs[q, r, :] * rs[q, pl.ds(s, 1), :]
+        hid = (u + mix[q, r, :]).astype(BF16).astype(F32)
+        pab[r, lanes] = (state * (u - dec[q, r, :]) * rec[q, r, :]).astype(BF16)
+        pib[r, lanes] = (state * nrm[q, r, :]).astype(BF16)
+        gm[q, r, :] = state * ing[q, r, :]
+        gg[r, lanes] = (gt[q, r, :] * hid).astype(BF16)
+
+    def back_maps(r, count):
+        for g in range(chans // gw):
+            cols = slice(g * gw, (g + 1) * gw)
+            back = dot(pab[r : r + count, cols], bda[cols, :], ((1,), (1,)))
+            back = back + dot(pib[r : r + count, cols], bdi[cols, :], ((1,), (1,)))
+            for q in range(gw // LANES):
+                at = g * (gw // LANES) + q
+                gm[at, r : r + count, :] = (
+                    gm[at, r : r + count, :] + back[:, q * LANES : (q + 1) * LANES]
+                )
+
+    for q in range(nq):
+        grads(q, 0)
+    back_maps(0, HALO)
     head = pltpu.make_async_remote_copy(
         src_ref=gm.at[:, pl.ds(0, 8), :], dst_ref=gm.at[:, pl.ds(rows, 8), :],
         send_sem=head_sem.at[0], recv_sem=head_sem.at[1],
         device_id={"sp": lax.rem(me + n_sp - 1, n_sp)}, device_id_type=MESH,
     )
     head.start()
+    for q in range(nq):
+
+        def others(s, carry, q=q):
+            grads(q, s)
+            return carry
+
+        lax.fori_loop(1, SEGS, others, 0)
+    back_maps(HALO, rows - HALO)
     width = 512 if depth % 512 == 0 else depth
     for d in range(0, depth, width):
         acc[:, d : d + width] = dot(gg[...], wg[d : d + width, :], ((1,), (1,)))
@@ -345,7 +383,7 @@
     def product(k):
         zd = lax.rem(zi + k, last)
         at = pl.ds(pl.multiple_of(zd * wide, wide), wide)
-        prod = dot(xs[pl.ds(HALO, rows), at], gb[...], ((0,), (0,)))
+        prod = dot(xs[:, at], gb[...], ((0,), (0,)))
         for v in range(per_last):
             part[k, bitrev(v, bits)] = prod[v * share : (v + 1) * share].astype(BF16)
         if bits:
@@ -358,25 +396,32 @@
             tsend[k - 1, c] = term(lax.rem(tp + k, n_tp), c).astype(BF16)
             term_copy(k, c).start()
 
-    terms(0)
-    for k in order[:2]:
+    def stage(i, k):
+        size = 2 ** (bits - 1 - i)
+        stage_copy(i, k).wait_recv()
+        off = digit(i) * size
+        for v in range(size):
+            mine = part[k, off + v] if i == 0 else sacc[i - 1, k, off + v]
+            sacc[i, k, v] = (mine.astype(F32) + srecv[i, k, v].astype(F32)).astype(BF16)
+        if i + 1 < bits:
+            stage_copy(i + 1, k).start()
+        elif k:
+            last_copy(k).start()
+
+    todo = list(range(pieces))
+    for n, k in enumerate(order):
         product(k)
-    for c in range(1, pieces):
+        if todo:
+            terms(todo.pop(0))
+        if n and bits:
+            stage(0, order[n - 1])
+    for c in todo:
         terms(c)
-    for k in order[2:]:
-        product(k)
-    for i in range(bits):
-        size = 2 ** (bits - 1 - i)
+    if bits:
+        stage(0, order[-1])
+    for i in range(1, bits):
         for k in order:
-            stage_copy(i, k).wait_recv()
-            off = digit(i) * size
-            for v in range(size):
-                mine = part[k, off + v] if i == 0 else sacc[i - 1, k, off + v]
-                sacc[i, k, v] = (mine.astype(F32) + srecv[i, k, v].astype(F32)).astype(BF16)
-            if i + 1 < bits:
-                stage_copy(i + 1, k).start()
-            elif k:
-                last_copy(k).start()
+            stage(i, k)
     for c in range(pieces):
         tsend[n_tp - 1, c] = term(tp, c).astype(BF16)
     total = (part[0, 0] if bits == 0 else sacc[bits - 1, 0, 0]).astype(F32)
@@ -404,6 +449,15 @@
     for c in range(pieces):
         for k in range(1, n_tp):
             term_copy(k, c).wait_send()
+
+
+def put_out(gin, gproj, gin_out, gproj_out, sem):
+    one = pltpu.make_async_copy(gin, gin_out, sem.at[0])
+    two = pltpu.make_async_copy(gproj, gproj_out, sem.at[1])
+    one.start()
+    two.start()
+    one.wait()
+    two.wait()
 
 
 def body(n_sp, n_tp, block_input, proj_x, proj_gate, conv_taps, gate_a, gate_in, decay_param,
@@ -425,7 +479,8 @@
     anywhere = pl.BlockSpec(memory_space=pl.ANY)
     local = pl.BlockSpec(memory_space=pltpu.VMEM)
     scratch = [
-        vm((rows + HALO, depth), BF16), vm((depth, chans), BF16), vm((depth, chans), BF16),
+        vm(conv_taps.shape, F32), vm(gate_a.shape, BF16), vm(gate_in.shape, BF16), vm((1, chans), F32),
+        vm((rows, depth), BF16), vm((depth, chans), BF16), vm((depth, chans), BF16),
         vm((rows, chans), F32), vm((rows, chans), BF16),
         grid_f32, vm((nq, rows + HALO, LANES), F32), grid_f32, vm((rows, chans), BF16),
         vm((chans, gw), BF16), vm((chans, gw), BF16),
@@ -440,17 +495,14 @@
         vm((stages, last, most, share, chans), BF16),
         vm((stages, last, most, share, chans), BF16),
         vm((last, share, chans), BF16),
-        dma((5,)), dma((2,)), dma((n_sp,)), dma((n_sp,)), dma((2,)),
+        dma((9,)), dma((2,)), dma((n_sp,)), dma((n_sp,)), dma((2,)),
         dma((n_tp, pieces)), dma((n_tp, pieces)), dma((stages, last)), dma((stages, last)),
         dma((last,)), dma((last,)),
     ]
-    return pl.pallas_call(
+    held = pl.pallas_call(
         functools.partial(kernel, n_sp, n_tp),
-        out_shape=(
-            jax.ShapeDtypeStruct((own, depth), BF16),
-            jax.ShapeDtypeStruct((share, chans), F32),
-        ),
-        in_specs=[anywhere] * 3 + [local] * 4 + [anywhere] * 2,
+        out_shape=(vm((own, depth), BF16), vm((share, chans), F32)),
+        in_specs=[anywhere] * 9,
         out_specs=(local, local),
         scratch_shapes=scratch,
         compiler_params=pltpu.CompilerParams(
@@ -458,6 +510,17 @@
         ),
     )(block_input, proj_x, proj_gate, conv_taps, gate_a, gate_in, decay_param.reshape(1, chans),
       log_jump, out_grad)
+    return pl.pallas_call(
+        put_out,
+        out_shape=(
+            jax.ShapeDtypeStruct((own, depth), BF16),
+            jax.ShapeDtypeStruct((share, chans), F32),
+        ),
+        in_specs=[local] * 2,
+        out_specs=(anywhere, anywhere),
+        scratch_shapes=[dma((2,))],
+        compiler_params=pltpu.CompilerParams(vmem_limit_bytes=4 * 1024 * 1024),
+    )(*held)
 
 
 def solution(mesh):

time: 51.2 us -> 42.5 us (0.83)
  Pallas kernels: 46.6 us -> 41.7 us
  local copies, waits for them, and re-layouts: 3.76 us -> 0 us
    pallas_call x1 -> x2, Pallas kernels: 46.6 us -> 41.7 us  [the longest x1 40.8 us: body(): pl.pallas_call(functools.partial(kernel, n_sp, n_tp), out_shape=(vm((own,...]
    unnamed x2 -> x0, local copies, waits for them, and re-layouts: 3.76 us -> none
where the time goes in v2:
time: 42.5 us; the launch traced here: 42.4 us
  Pallas kernels  41.7 us (98%)
  between operations  0.64 us (2%)
    pallas_call x1, Pallas kernels, body(): pl.pallas_call(functools.partial(kernel, n_sp, n_tp), out_shape=(vm((own,...  40.8 us
    pallas_call x1, Pallas kernels, body(): pl.pallas_call(put_out, out_shape=(jax.ShapeDtypeStruct((own, depth), BF1...  0.98 us

profile of v2, /device:TPU:0, one launch (start us, length us, event | category | flops | bytes accessed | tf_op | source)
XLA Modules:
  0.0 42.4 jit_solution(12247980866399540751)
XLA Ops:
  0.6 40.8 %shard_map.104 = (bf16[192,2048]{1,0:T(8,128)(2,1)S(1)}, f32[128,512]{1,0:T(8,128)S(1)}) custom-call(bf16[384,2048]{1,0:T(8,128)(2,1)} %x_hbm.1, bf16[2048,512]{1,0:T(8,128)(2,1)} %wx_hbm.1, bf16[2048,512]{1,0:T(8,128)(2,1)} %wg_hbm.1, f32[4,512]{1,0:T(4,128)} %taps_hbm.1, bf16[8,64,64]{2,1,0:T(8,128)(2,1)} %ga_hbm.1, bf16[8,64,64]{2,1,0:T(8,128)(2,1)} %gi_hbm.1, ...), custom_call_target="tpu_custom_call" | custom-call | tf_op jit(solution)/shard_map/pallas_call | solution.py:502
  41.4 1.0 %shard_map.105 = (bf16[192,2048]{1,0:T(8,128)(2,1)}, f32[128,512]{1,0:T(8,128)}) custom-call(bf16[192,2048]{1,0:T(8,128)(2,1)S(1)} %get-tuple-element.4.gin, f32[128,512]{1,0:T(8,128)S(1)} %get-tuple-element.5.gproj), custom_call_target="tpu_custom_call" | custom-call | tf_op jit(solution)/shard_map/pallas_call | solution.py:513

commit v3 on v2

--- a/solution.py
+++ b/solution.py
@@ -58,7 +58,7 @@
     n_sp, n_tp, x_hbm, wx_hbm, wg_hbm, taps_hbm, ga_hbm, gi_hbm, dp_hbm, lj_hbm, og_hbm,
     gin_out, gproj_out,
     taps, ga, gi, dp, xs, wx, wg, lj, og, gt, br, mix, mixb, bda, bdi, rec, ing, dec, nrm, us, ps, gs, qs,
-    cs, rs, sbuf, rbuf, pab, pib, gg, gm, gb, acc, tsend, trecv, part, srecv, sacc, lrecv,
+    cs, rs, sbuf, rbuf, pab, pib, gg, gm, gb, wgt, wxt, xt, tsend, trecv, part, srecv, sacc, lrecv,
     loc_sem, halo_sem, msend_sem, mrecv_sem, head_sem, tsend_sem, trecv_sem, ssend_sem,
     srecv_sem, lsend_sem, lrecv_sem,
 ):
@@ -208,7 +208,7 @@
 
     zero = jnp.zeros((SEGS, LANES), F32)
     one = jnp.ones((SEGS, LANES), F32)
-    ends = lax.fori_loop(0, seg, scan, tuple((zero, one, zero, one) for _ in range(nq)), unroll=2)
+    ends = lax.fori_loop(0, seg, scan, tuple((zero, one, zero, one) for _ in range(nq)), unroll=4)
     for q in range(nq):
         h, p, g, _ = ends[q]
         fwd = jnp.zeros((1, LANES), F32)
@@ -260,6 +260,9 @@
             return carry
 
         lax.fori_loop(0, rows // sub, ready, 0)
+    wgt[...] = wg[...].T
+    wxt[...] = wx[...].T
+    xt[...] = xs[...].T
     for c in sent:
         c.wait_recv()
     fwd = jnp.zeros((nq, LANES), F32)
@@ -318,21 +321,45 @@
 
         lax.fori_loop(1, SEGS, others, 0)
     back_maps(HALO, rows - HALO)
-    width = 512 if depth % 512 == 0 else depth
-    for d in range(0, depth, width):
-        acc[:, d : d + width] = dot(gg[...], wg[d : d + width, :], ((1,), (1,)))
+    def convolve_back(r, end):
+        for q in range(nq):
+            lanes = slice(q * LANES, (q + 1) * LANES)
+            total = jnp.zeros((end - r, LANES), F32)
+            for j in range(taps_n):
+                off = taps_n - 1 - j
+                total = total + taps[j : j + 1, lanes] * gm[q, r + off : end + off, :]
+            gb[r:end, lanes] = total.astype(BF16)
+
+    own = rows // n_tp
+    pieces = tsend.shape[1]
+    piece = own // pieces
+
+    def term(at, c):
+        r = pl.ds(pl.multiple_of(at * own + c * piece, piece), piece)
+        return dot(gg[r, :], wgt[...]) + dot(gb[r, :], wxt[...])
+
+    def term_copy(k, c):
+        return pltpu.make_async_remote_copy(
+            src_ref=tsend.at[k - 1, c], dst_ref=trecv.at[k - 1, c],
+            send_sem=tsend_sem.at[k - 1, c], recv_sem=trecv_sem.at[k - 1, c],
+            device_id={"tp": lax.rem(tp + k, n_tp)}, device_id_type=MESH,
+        )
+
+    def terms(c):
+        for k in range(1, n_tp):
+            tsend[k - 1, c] = term(lax.rem(tp + k, n_tp), c).astype(BF16)
+            term_copy(k, c).start()
+
+    todo = list(range(pieces))
+    for r in range(0, rows - HALO, step):
+        convolve_back(r, min(r + step, rows - HALO))
+    if pieces > 1:
+        terms(todo.pop(0))
     head.wait_recv()
     final = me == n_sp - 1
     for q in range(nq):
         gm[q, rows : rows + 8, :] = jnp.where(final, 0.0, gm[q, rows : rows + 8, :])
-    for q in range(nq):
-        lanes = slice(q * LANES, (q + 1) * LANES)
-        for r in range(0, rows, step):
-            total = jnp.zeros((step, LANES), F32)
-            for j in range(taps_n):
-                off = taps_n - 1 - j + r
-                total = total + taps[j : j + 1, lanes] * gm[q, off : off + step, :]
-            gb[r : r + step, lanes] = total.astype(BF16)
+    convolve_back(rows - HALO, rows)
 
     order = list(range(1, last)) + [0]
     wide = depth // last
@@ -364,37 +391,16 @@
             device_id={"sp": lax.rem(zi + k, last) * per_last + inner}, device_id_type=MESH,
         )
 
-    own = rows // n_tp
-    pieces = tsend.shape[1]
-    piece = depth // pieces
-
-    def term(at, c):
-        r = pl.ds(pl.multiple_of(at * own, own), own)
-        cols = slice(c * piece, (c + 1) * piece)
-        return acc[r, cols] + dot(gb[r, :], wx[cols, :], ((1,), (1,)))
-
-    def term_copy(k, c):
-        return pltpu.make_async_remote_copy(
-            src_ref=tsend.at[k - 1, c], dst_ref=trecv.at[k - 1, c],
-            send_sem=tsend_sem.at[k - 1, c], recv_sem=trecv_sem.at[k - 1, c],
-            device_id={"tp": lax.rem(tp + k, n_tp)}, device_id_type=MESH,
-        )
-
     def product(k):
         zd = lax.rem(zi + k, last)
         at = pl.ds(pl.multiple_of(zd * wide, wide), wide)
-        prod = dot(xs[:, at], gb[...], ((0,), (0,)))
+        prod = dot(xt[at, :], gb[...])
         for v in range(per_last):
             part[k, bitrev(v, bits)] = prod[v * share : (v + 1) * share].astype(BF16)
         if bits:
             stage_copy(0, k).start()
         elif k:
             last_copy(k).start()
-
-    def terms(c):
-        for k in range(1, n_tp):
-            tsend[k - 1, c] = term(lax.rem(tp + k, n_tp), c).astype(BF16)
-            term_copy(k, c).start()
 
     def stage(i, k):
         size = 2 ** (bits - 1 - i)
@@ -408,21 +414,22 @@
         elif k:
             last_copy(k).start()
 
-    todo = list(range(pieces))
     for n, k in enumerate(order):
         product(k)
-        if todo:
-            terms(todo.pop(0))
         if n and bits:
             stage(0, order[n - 1])
+    if bits:
+        stage(0, order[-1])
     for c in todo:
         terms(c)
-    if bits:
-        stage(0, order[-1])
+    mine = list(range(pieces))
     for i in range(1, bits):
         for k in order:
             stage(i, k)
-    for c in range(pieces):
+            if mine:
+                c = mine.pop(0)
+                tsend[n_tp - 1, c] = term(tp, c).astype(BF16)
+    for c in mine:
         tsend[n_tp - 1, c] = term(tp, c).astype(BF16)
     total = (part[0, 0] if bits == 0 else sacc[bits - 1, 0, 0]).astype(F32)
     for k in range(1, last):
@@ -430,12 +437,11 @@
         total = total + lrecv[k].astype(F32)
     gproj_out[...] = total
     for c in range(pieces):
-        cols = slice(c * piece, (c + 1) * piece)
         total = tsend[n_tp - 1, c].astype(F32)
         for k in range(1, n_tp):
             term_copy(k, c).wait_recv()
             total = total + trecv[k - 1, c].astype(F32)
-        gin_out[:, cols] = total.astype(BF16)
+        gin_out[c * piece : (c + 1) * piece, :] = total.astype(BF16)
 
     halo.wait_send()
     head.wait_send()
@@ -470,7 +476,7 @@
     per_last = n_sp // last
     share = depth // n_sp
     own = rows // n_tp
-    pieces = 2
+    pieces = 2 if own % 32 == 0 else 1
     stages = max(bits, 1)
     most = max(per_last // 2, 1)
     vm = pltpu.VMEM
@@ -488,9 +494,10 @@
         vm((nq, SEGS, LANES), F32), vm((nq, SEGS, LANES), F32),
         vm((2, 2 * nq, LANES), F32), vm((n_sp, 2 * nq, LANES), F32),
         vm((rows, chans), BF16), vm((rows, chans), BF16), vm((rows, chans), BF16),
-        vm((nq, rows + 8, LANES), F32), vm((rows, chans), BF16), vm((rows, depth), F32),
-        vm((n_tp, pieces, own, depth // pieces), BF16),
-        vm((max(n_tp - 1, 1), pieces, own, depth // pieces), BF16),
+        vm((nq, rows + 8, LANES), F32), vm((rows, chans), BF16),
+        vm((chans, depth), BF16), vm((chans, depth), BF16), vm((depth, rows), BF16),
+        vm((n_tp, pieces, own // pieces, depth), BF16),
+        vm((max(n_tp - 1, 1), pieces, own // pieces, depth), BF16),
         vm((last, per_last, share, chans), BF16),
         vm((stages, last, most, share, chans), BF16),
         vm((stages, last, most, share, chans), BF16),

time: 42.5 us -> 41.1 us (0.967)
  Pallas kernels: 41.7 us -> 40.3 us
    pallas_call x1, Pallas kernels: 40.8 us -> 39.4 us  [body(): pl.pallas_call(functools.partial(kernel, n_sp, n_tp), out_shape=(vm((own,...]
where the time goes in v3:
time: 41.1 us; the launch traced here: 41 us
  Pallas kernels  40.3 us (98%)
  between operations  0.64 us (2%)
    pallas_call x1, Pallas kernels, body(): pl.pallas_call(functools.partial(kernel, n_sp, n_tp), out_shape=(vm((own,...  39.4 us
    pallas_call x1, Pallas kernels, body(): pl.pallas_call(put_out, out_shape=(jax.ShapeDtypeStruct((own, depth), BF1...  0.98 us

profile of v3, /device:TPU:0, one launch (start us, length us, event | category | flops | bytes accessed | tf_op | source)
XLA Modules:
  0.0 41.0 jit_solution(17854520768217157428)
XLA Ops:
  0.6 39.4 %shard_map.104 = (bf16[192,2048]{1,0:T(8,128)(2,1)S(1)}, f32[128,512]{1,0:T(8,128)S(1)}) custom-call(bf16[384,2048]{1,0:T(8,128)(2,1)} %x_hbm.1, bf16[2048,512]{1,0:T(8,128)(2,1)} %wx_hbm.1, bf16[2048,512]{1,0:T(8,128)(2,1)} %wg_hbm.1, f32[4,512]{1,0:T(4,128)} %taps_hbm.1, bf16[8,64,64]{2,1,0:T(8,128)(2,1)} %ga_hbm.1, bf16[8,64,64]{2,1,0:T(8,128)(2,1)} %gi_hbm.1, ...), custom_call_target="tpu_custom_call" | custom-call | tf_op jit(solution)/shard_map/pallas_call | solution.py:509
  40.0 1.0 %shard_map.105 = (bf16[192,2048]{1,0:T(8,128)(2,1)}, f32[128,512]{1,0:T(8,128)}) custom-call(bf16[192,2048]{1,0:T(8,128)(2,1)S(1)} %get-tuple-element.4.gin, f32[128,512]{1,0:T(8,128)S(1)} %get-tuple-element.5.gproj), custom_call_target="tpu_custom_call" | custom-call | tf_op jit(solution)/shard_map/pallas_call | solution.py:520
